TPU v7x, 32 devices: a whole 2x2x4 slice. The times are simulated.
32 devices in a mesh: fs: 16 (over z, y, x), tp: 2 (over core).
Axes of the slice: x: 2, y: 2, z: 4, core: 2. Of those that a mesh axis runs over, the one named last changes fastest.
Arguments:
- tokens: bfloat16 [2048, 2048], P('fs'), may hold values from -6 to 6
- norm_gain: float32 [2048], replicated, may hold values from 0.1 to 1.9
- w_query: bfloat16 [2048, 1024], P('fs', 'tp'), may hold values from -0.125 to 0.125
- w_key: bfloat16 [2048, 1024], P('fs', 'tp'), may hold values from -0.125 to 0.125
- w_value: bfloat16 [2048, 2048], P('fs', 'tp'), may hold values from -0.125 to 0.125
- w_gate: bfloat16 [2048, 2048], P('fs', 'tp'), may hold values from -0.125 to 0.125
- mixer_gain: float32 [2048], P('tp'), may hold values from 0.1 to 1.9
- w_out: bfloat16 [2048, 2048], P('tp', 'fs'), may hold values from -0.125 to 0.125
- channel_gain: float32 [2048], replicated, may hold values from 0.1 to 1.9
- w_left: bfloat16 [2048, 3072], P('fs', 'tp'), may hold values from -0.125 to 0.125
- w_right: bfloat16 [2048, 3072], P('fs', 'tp'), may hold values from -0.125 to 0.125
- taps_left: float32 [3, 3072], P(None, 'tp'), may hold values from -3.5 to 3.5
- taps_right: float32 [3, 3072], P(None, 'tp'), may hold values from -3.5 to 3.5
- w_down: bfloat16 [3072, 2048], P('tp', 'fs'), may hold values from -0.109375 to 0.109375
Outputs:
- layer_out: bfloat16 [2048, 2048], P('fs')
All inputs are finite; a program needn't handle non-finite values.
Results may differ from a plain program's by a relative error of at most 0.018.
Values may be sent and summed in bfloat16 or wider, within the bound.
A program may use at most 64 MiB of HBM per device.

v0:
```python
import jax
import jax.numpy as jnp
from jax import lax
from jax.sharding import PartitionSpec as P

DK = 128
DV = 256
BLOCK = 128


highest = lax.Precision.HIGHEST


def scale_rows(rows_in, gain_vec):
    floats = rows_in.astype(jnp.float32)
    factor = lax.rsqrt(jnp.mean(floats * floats, axis=-1, keepdims=True) + 1e-06)
    return (floats * factor * gain_vec).astype(jnp.bfloat16)


def decays(first_head, count):
    head_ids = first_head + jnp.arange(count, dtype=jnp.float32)
    return jnp.log(1.0 - 2.0 ** (-5.0 - head_ids))


def rotate(heads_in, positions):
    width = heads_in.shape[-1]
    half = width // 2
    freqs = 10000.0 ** (-jnp.arange(half, dtype=jnp.float32) / half)
    angles = positions[:, None] * freqs[None, :]
    cosine = jnp.cos(angles)
    sine = jnp.sin(angles)
    first_half = heads_in[..., :half]
    second_half = heads_in[..., half:]
    return jnp.concatenate(
        [first_half * cosine - second_half * sine, first_half * sine + second_half * cosine],
        axis=-1,
    )


def retention(queries, keys_in, values_in, log_gamma):
    head_count, length, key_width = queries.shape
    value_width = values_in.shape[-1]
    blocks = length // BLOCK
    queries = queries.reshape(head_count, blocks, BLOCK, key_width)
    keys_in = keys_in.reshape(head_count, blocks, BLOCK, key_width)
    values_in = values_in.reshape(head_count, blocks, BLOCK, value_width)
    offsets = jnp.arange(BLOCK, dtype=jnp.float32)
    distance = offsets[:, None] - offsets[None, :]
    weights = jnp.where(
        distance >= 0, jnp.exp(log_gamma[:, None, None] * jnp.maximum(distance, 0.0)), 0.0
    )
    scores = jnp.einsum("hbnd,hbmd->hbnm", queries, keys_in, precision=highest) * weights[:, None]
    inner = jnp.einsum("hbnm,hbme->hbne", scores, values_in, precision=highest)
    key_weight = jnp.exp(log_gamma[:, None] * (BLOCK - 1 - offsets)[None, :])
    contrib = jnp.einsum(
        "hbjd,hbje->hbde", keys_in * key_weight[:, None, :, None], values_in, precision=highest
    )
    block_decay = jnp.exp(log_gamma * BLOCK)[:, None, None]

    def advance(state, contrib_block):
        return (state * block_decay + contrib_block, state)

    _, states = lax.scan(
        advance,
        jnp.zeros((head_count, key_width, value_width), jnp.float32),
        jnp.moveaxis(contrib, 1, 0),
    )
    states = jnp.moveaxis(states, 0, 1)
    query_weight = jnp.exp(log_gamma[:, None] * (offsets + 1.0)[None, :])
    carried = (
        jnp.einsum("hbnd,hbde->hbne", queries, states, precision=highest)
        * query_weight[:, None, :, None]
    )
    return (inner + carried).reshape(head_count, length, value_width)


def head_norm(retained):
    return retained * lax.rsqrt(jnp.mean(retained * retained, axis=-1, keepdims=True) + 1e-06)


def causal_taps(values_in, taps):
    length = values_in.shape[-2]
    padded = jnp.pad(values_in.astype(jnp.float32), ((taps.shape[0] - 1, 0), (0, 0)))
    result = padded[0:length] * taps[0]
    for tap_index in range(1, taps.shape[0]):
        result = result + padded[tap_index : tap_index + length] * taps[tap_index]
    return result


def fold_single(source, weight_piece):
    return jnp.dot(source, weight_piece, preferred_element_type=jnp.float32)


def collect_single(source, weight):
    return fold_single(source, lax.all_gather(weight, "fs", axis=0, tiled=True))


def body(
    tokens,
    norm_gain,
    w_query,
    w_key,
    w_value,
    w_gate,
    mixer_gain,
    w_out,
    channel_gain,
    w_left,
    w_right,
    taps_left,
    taps_right,
    w_down,
):
    length = tokens.shape[0]
    normed = scale_rows(tokens, norm_gain)
    queries = collect_single(normed, w_query)
    keys_proj = collect_single(normed, w_key)
    values_proj = collect_single(normed, w_value)
    gates = collect_single(normed, w_gate)
    queries = queries.astype(jnp.bfloat16)
    keys_proj = keys_proj.astype(jnp.bfloat16)
    values_proj = values_proj.astype(jnp.bfloat16)
    gates = gates.astype(jnp.bfloat16)
    heads_here = w_query.shape[1] // DK
    first_head = (lax.axis_index("tp") * heads_here).astype(jnp.float32)
    log_gamma = decays(first_head, heads_here)
    positions = jnp.arange(length, dtype=jnp.float32)

    def split_heads(rows_in, width):
        return rows_in.astype(jnp.float32).reshape(length, heads_here, width).transpose(1, 0, 2)

    retained = head_norm(
        retention(
            rotate(split_heads(queries, DK), positions),
            rotate(split_heads(keys_proj, DK), positions),
            split_heads(values_proj, DV),
            log_gamma,
        )
    )
    retained = retained.transpose(1, 0, 2).reshape(length, heads_here * DV)
    hidden = (retained * mixer_gain * jax.nn.silu(gates.astype(jnp.float32))).astype(jnp.bfloat16)
    rows_own = length // lax.axis_size("tp")
    first_row = lax.axis_index("tp") * rows_own
    out_whole = lax.all_gather(w_out, "fs", axis=1, tiled=True)
    mixer_total = lax.psum_scatter(
        jnp.dot(hidden, out_whole, preferred_element_type=jnp.float32).astype(jnp.bfloat16),
        "tp",
        scatter_dimension=0,
        tiled=True,
    ).astype(jnp.float32)
    residual = lax.dynamic_slice_in_dim(tokens, first_row, rows_own, 0)
    middle_own = (residual.astype(jnp.float32) + mixer_total).astype(jnp.bfloat16)
    middle = lax.all_gather(middle_own, "tp", axis=0, tiled=True)
    normed_mid = scale_rows(middle, channel_gain)
    left = collect_single(normed_mid, w_left)
    right = collect_single(normed_mid, w_right)
    left = left.astype(jnp.bfloat16)
    right = right.astype(jnp.bfloat16)
    gated = (jax.nn.silu(causal_taps(left, taps_left)) * causal_taps(right, taps_right)).astype(
        jnp.bfloat16
    )
    down_whole = lax.all_gather(w_down, "fs", axis=1, tiled=True)
    channel_part = jnp.dot(gated, down_whole, preferred_element_type=jnp.float32)
    channel_total = lax.psum(channel_part.astype(jnp.bfloat16), "tp").astype(jnp.float32)
    return (middle.astype(jnp.float32) + channel_total).astype(jnp.bfloat16)


def solution(mesh):
    placed = (
        P("fs", None),
        P(),
        P("fs", "tp"),
        P("fs", "tp"),
        P("fs", "tp"),
        P("fs", "tp"),
        P("tp"),
        P("tp", "fs"),
        P(),
        P("fs", "tp"),
        P("fs", "tp"),
        P(None, "tp"),
        P(None, "tp"),
        P("tp", "fs"),
    )
    return jax.shard_map(body, mesh=mesh, in_specs=placed, out_specs=P("fs", None), check_vma=False)
```

profile of v0, /device:TPU:0, one launch (start us, length us, event | category | flops | bytes accessed | tf_op | source)
XLA Modules:
  0.0 730.4 jit_solution(5038678450189377104)
XLA Ops:
  6.5 0.7 all-gather.11.cloned.1.call-update
  7.3 0.7 all-gather.9.cloned.1.call-update
  10.1 1.2 fusion.7
  11.7 61.5 %all-gather.11.cloned.1.call-done = bf16[2048,512]{1,0:T(8,128)(2,1)} async-done(((bf16[128,512]{1,0:T(8,128)(2,1)}), bf16[2048,512]{1,0:T(8,128)(2,1)}) %all-gather.11.cloned.1.call-update) | async-done | bytes 2097168 | tf_op jit(solution)/shard_map/all_gather | solution.py:95
  73.2 2.3 fusion.4
  75.5 59.7 %all-gather.9.cloned.1.call-done = bf16[2048,512]{1,0:T(8,128)(2,1)} async-done(((bf16[128,512]{1,0:T(8,128)(2,1)}), bf16[2048,512]{1,0:T(8,128)(2,1)}) %all-gather.9.cloned.1.call-update) | async-done | bytes 2097168 | tf_op jit(solution)/shard_map/all_gather | solution.py:95
  135.2 2.1 fusion.6
  138.1 0.7 convolution_multiply_fusion
  138.8 73.6 %all-gather.13.cloned.1.call-done = bf16[2048,1024]{1,0:T(8,128)(2,1)} async-done(((bf16[128,1024]{1,0:T(8,128)(2,1)}), bf16[2048,1024]{1,0:T(8,128)(2,1)}) %all-gather.13.cloned.1.call-update) | async-done | bytes 4194320 | tf_op jit(solution)/shard_map/all_gather | solution.py:95
  212.4 2.9 convolution_convert_fusion.5
  216.5 72.8 %all-gather.15.cloned.1.call-done = bf16[2048,1024]{1,0:T(8,128)(2,1)} async-done(((bf16[128,1024]{1,0:T(8,128)(2,1)}), bf16[2048,1024]{1,0:T(8,128)(2,1)}) %all-gather.15.cloned.1.call-update) | async-done | bytes 4194320 | tf_op jit(solution)/shard_map/all_gather | solution.py:95
  289.3 89.9 %all-gather.17.cloned.1.call-done = bf16[1024,2048]{1,0:T(8,128)(2,1)} async-done(((bf16[1024,128]{1,0:T(8,128)(2,1)}), bf16[1024,2048]{1,0:T(8,128)(2,1)}) %all-gather.17.cloned.1.call-update) | async-done | bytes 4194320 | tf_op jit(solution)/shard_map/all_gather | solution.py:144
  379.2 5.7 convolution_convert_fusion.1
  387.3 3.9 reduce-scatter.2.cloned.1.call-done
  391.2 1.0 add_convert_fusion
  392.2 2.2 all_gather.32
  394.5 93.9 %all-gather.19.cloned.1.call-done = bf16[2048,1536]{1,0:T(8,128)(2,1)} async-done(((bf16[128,1536]{1,0:T(8,128)(2,1)}), bf16[2048,1536]{1,0:T(8,128)(2,1)}) %all-gather.19.cloned.1.call-update) | async-done | bytes 6291472 | tf_op jit(solution)/shard_map/all_gather | solution.py:95
  488.5 3.8 fusion.1
  492.3 90.9 %all-gather.21.cloned.1.call-done = bf16[2048,1536]{1,0:T(8,128)(2,1)} async-done(((bf16[128,1536]{1,0:T(8,128)(2,1)}), bf16[2048,1536]{1,0:T(8,128)(2,1)}) %all-gather.21.cloned.1.call-update) | async-done | bytes 6291472 | tf_op jit(solution)/shard_map/all_gather | solution.py:95
  583.2 3.8 fusion
  587.0 112.5 %all-gather.23.cloned.1.call-done = bf16[1536,2048]{1,0:T(8,128)(2,1)} async-done(((bf16[1536,128]{1,0:T(8,128)(2,1)}), bf16[1536,2048]{1,0:T(8,128)(2,1)}) %all-gather.23.cloned.1.call-update) | async-done | bytes 6291472 | tf_op jit(solution)/shard_map/all_gather | solution.py:162
  699.5 5.1 convolution_convert_fusion
  704.6 16.9 %all-reduce.4.cloned.1.call-done = bf16[128,2048]{1,0:T(8,128)(2,1)} async-done(((bf16[128,2048]{1,0:T(8,128)(2,1)}), bf16[128,2048]{1,0:T(8,128)(2,1)}) %all-reduce.4.cloned.1.call-update) | async-done | bytes 524304 | tf_op jit(solution)/shard_map/psum | solution.py:164
  721.6 2.0 fusion.13
  (51 shorter events, 6.9 us)
Async XLA Ops:
  6.5 128.7 %copy-start = (bf16[128,2048]{1,0:T(8,128)(2,1)S(1)}, bf16[128,2048]{1,0:T(8,128)(2,1)}, u32[]{:S(2)}) copy-start(bf16[128,2048]{1,0:T(8,128)(2,1)} %param.14) | copy-start | bytes 1572868
  6.5 128.7 %copy-start.1 = (f32[2048]{0:T(1024)S(1)}, f32[2048]{0:T(1024)}, u32[]{:S(2)}) copy-start(f32[2048]{0:T(1024)} %param.15) | copy-start | bytes 24580
  6.5 66.7 %all-gather.11.cloned.1.call-start = ((), (), s32[]{:S(2)}) async-start(), calls=%async_computation.2 | async-start | bytes 2228224 | tf_op jit(solution)/shard_map/all_gather | solution.py:95
  7.3 128.0 %all-gather.9.cloned.1.call-start = ((), (), s32[]{:S(2)}) async-start(), calls=%async_computation.1 | async-start | bytes 2228224 | tf_op jit(solution)/shard_map/all_gather | solution.py:95
  8.0 204.4 %all-gather.13.cloned.1.call-start = ((), (), s32[]{:S(2)}) async-start(), calls=%async_computation.3 | async-start | bytes 4456448 | tf_op jit(solution)/shard_map/all_gather | solution.py:95
  8.7 280.5 %all-gather.15.cloned.1.call-start = ((), (), s32[]{:S(2)}) async-start(), calls=%async_computation.4 | async-start | bytes 4456448 | tf_op jit(solution)/shard_map/all_gather | solution.py:95
  9.3 369.8 %all-gather.17.cloned.1.call-start = ((), (), s32[]{:S(2)}) async-start(), calls=%async_computation.5 | async-start | bytes 4456448 | tf_op jit(solution)/shard_map/all_gather | solution.py:144
  9.9 381.2 %reduce-scatter.2.cloned.1.call-start = ((), (), s32[]{:S(2)}) async-start(), calls=%async_computation.6 | async-start | bytes 786432 | tf_op jit(solution)/shard_map/reduce_scatter | solution.py:145
  138.8 240.4 %copy-start.5 = (f32[1024]{0:T(1024)S(1)}, f32[1024]{0:T(1024)}, u32[]{:S(2)}) copy-start(f32[1024]{0:T(1024)} %param.20) | copy-start | bytes 12292
  216.5 170.7 %copy-start.3 = (f32[3,1536]{1,0:T(4,128)S(1)}, f32[3,1536]{1,0:T(4,128)}, u32[]{:S(2)}) copy-start(f32[3,1536]{1,0:T(4,128)} %param.26) | copy-start | bytes 55300
  216.5 170.7 %copy-start.4 = (f32[3,1536]{1,0:T(4,128)S(1)}, f32[3,1536]{1,0:T(4,128)}, u32[]{:S(2)}) copy-start(f32[3,1536]{1,0:T(4,128)} %param.25) | copy-start | bytes 55300
  216.5 272.0 %copy-start.2 = (f32[2048]{0:T(1024)S(1)}, f32[2048]{0:T(1024)}, u32[]{:S(2)}) copy-start(f32[2048]{0:T(1024)} %param.22) | copy-start | bytes 24580
  384.9 103.6 %all-gather.19.cloned.1.call-start = ((), (), s32[]{:S(2)}) async-start(), calls=%async_computation.7 | async-start | bytes 6684672 | tf_op jit(solution)/shard_map/all_gather | solution.py:95
  385.6 197.6 %all-gather.21.cloned.1.call-start = ((), (), s32[]{:S(2)}) async-start(), calls=%async_computation.8 | async-start | bytes 6684672 | tf_op jit(solution)/shard_map/all_gather | solution.py:95
  386.4 313.1 %all-gather.23.cloned.1.call-start = ((), (), s32[]{:S(2)}) async-start(), calls=%async_computation.9 | async-start | bytes 6684672 | tf_op jit(solution)/shard_map/all_gather | solution.py:162
  387.1 334.4 %all-reduce.4.cloned.1.call-start = ((), (), s32[]{:S(2)}) async-start(), calls=%async_computation.10 | async-start | bytes 1048576 | tf_op jit(solution)/shard_map/psum | solution.py:164
Sparse Core Ops, SparseCore 0:
  10.1 63.0 all-gather.10
  76.0 59.1 all-gather.8
  138.0 74.3 all-gather.12
  215.0 74.1 all-gather.14
  291.8 87.3 all-gather.16
  385.0 6.0 reduce-scatter.1
  393.9 94.5 all-gather.18
  491.3 91.9 all-gather.20
  585.9 113.5 all-gather.22
  704.8 16.7 all-reduce.3
where the time goes:
time: 731 us; the launch traced here: 730 us
  waiting for transfers between devices  681 us (93%)
  matrix products  27.3 us (4%)
  between operations  13.7 us (2%)
    all_gather x6, waiting for transfers between devices, collect_single(): return fold_single(source, lax.all_gather(weight, 'fs', axis=0, tiled=True))  452 us
    all_gather x1, waiting for transfers between devices, body(): down_whole = lax.all_gather(w_down, 'fs', axis=1, tiled=True)  112 us
    all_gather x1, waiting for transfers between devices, body(): out_whole = lax.all_gather(w_out, 'fs', axis=1, tiled=True)  89.9 us
    psum x1, waiting for transfers between devices, body(): lax.psum(channel_part.astype(jnp.bfloat16), 'tp').astype(jnp.float32)  16.9 us
    dot_general x5, matrix products, fold_single(): return jnp.dot(source, weight_piece, preferred_element_type=jnp.float32)  14.9 us
  transfers between devices with their start and end apart: 10, of which 10 were waited for; matrix products, arithmetic and copies ran while one was open for 3% of the time, Pallas kernels for 0%

commit v1 on v0

--- a/solution.py
+++ b/solution.py
@@ -1,11 +1,17 @@
+import functools
+
 import jax
 import jax.numpy as jnp
+import numpy as np
 from jax import lax
+from jax.experimental import pallas as pl
+from jax.experimental.pallas import tpu as pltpu
 from jax.sharding import PartitionSpec as P
 
 DK = 128
 DV = 256
 BLOCK = 128
+MESH = pl.DeviceIdType.MESH
 
 
 highest = lax.Precision.HIGHEST
@@ -95,7 +101,7 @@
     return fold_single(source, lax.all_gather(weight, "fs", axis=0, tiled=True))
 
 
-def body(
+def plain_body(
     tokens,
     norm_gain,
     w_query,
@@ -165,6 +171,415 @@
     return (middle.astype(jnp.float32) + channel_total).astype(jnp.bfloat16)
 
 
+def log_gammas(head_count):
+    table = np.log(1.0 - 2.0 ** (-5.0 - np.arange(head_count, dtype=np.float64)))
+    return np.repeat(table[:, None], BLOCK, axis=1).astype(np.float32)
+
+
+def turning(length, width):
+    half = width // 2
+    freqs = np.float32(10000.0) ** (-np.arange(half, dtype=np.float32) / np.float32(half))
+    angles = (np.arange(length, dtype=np.float32)[:, None] * freqs[None, :]).astype(np.float64)
+    cosine, sine = np.cos(angles), np.sin(angles)
+    return (
+        np.concatenate([cosine, cosine], axis=1).astype(np.float32),
+        np.concatenate([-sine, sine], axis=1).astype(np.float32),
+    )
+
+
+def silu(v):
+    return v / (1.0 + jnp.exp(-v))
+
+
+def normed_rows(floats, gain):
+    factor = lax.rsqrt(jnp.mean(floats * floats, axis=-1, keepdims=True) + 1e-06)
+    return (floats * factor * gain).astype(jnp.bfloat16)
+
+
+def layer_kernel(
+    n_fs,
+    groups,
+    tokens,
+    norm_gain,
+    wq,
+    wk,
+    wv,
+    wg,
+    mixer_gain,
+    wo,
+    channel_gain,
+    wl,
+    wr,
+    taps_left,
+    taps_right,
+    wd,
+    cos_t,
+    sin_t,
+    gammas,
+    out,
+    w1,
+    wout,
+    wlr,
+    wdown,
+    nt,
+    nm,
+    qkvg,
+    hid,
+    gated,
+    part1,
+    part2,
+    xb1,
+    xb2,
+    sb1,
+    sb2,
+    rb1,
+    rb2,
+    mid,
+    fin,
+    fin_in,
+    s1_send,
+    s1_recv,
+    self_sem,
+    s2_send,
+    s2_recv,
+    a_send,
+    a_recv,
+    f_send,
+    f_recv,
+    x_send,
+    x_recv,
+    r_send,
+    r_recv,
+    o_send,
+    o_recv,
+):
+    fs, tp = lax.axis_index("fs"), lax.axis_index("tp")
+    planes = n_fs // groups
+    z, q = fs // planes, lax.rem(fs, planes)
+    other = 1 - tp
+    length, width = tokens.shape
+    own = length // 2
+    kb = wq.shape[0]
+    nb = wo.shape[1]
+    cq, cv, cf = wq.shape[1] // groups, wv.shape[1] // groups, wl.shape[1] // groups
+
+    def zpeer(step):
+        return lax.rem(z + step, groups)
+
+    def zback(step):
+        return lax.rem(z + groups - step, groups)
+
+    def zdev(target):
+        return {"fs": target * planes + q, "tp": tp}
+
+    def qdev(step):
+        return {"fs": z * planes + lax.rem(q + step, planes), "tp": tp}
+
+    partner = {"fs": fs, "tp": other}
+
+    def lanes(index, size):
+        return pl.ds(pl.multiple_of(index * size, 128), size)
+
+    def rows(index, size):
+        return pl.ds(pl.multiple_of(index * size, size), size)
+
+    def region(cls, f):
+        if cls == 0:
+            return w1.at[rows(f, kb), :]
+        if cls == 1:
+            return wout.at[:, lanes(f, nb)]
+        if cls == 2:
+            return wlr.at[rows(f, kb), :]
+        return wdown.at[:, lanes(f, nb)]
+
+    pieces = (
+        (0, lambda c: wq.at[:, lanes(c, cq)], lambda f: w1.at[rows(f, kb), pl.ds(0, cq)]),
+        (0, lambda c: wk.at[:, lanes(c, cq)], lambda f: w1.at[rows(f, kb), pl.ds(cq, cq)]),
+        (0, lambda c: wv.at[:, lanes(c, cv)], lambda f: w1.at[rows(f, kb), pl.ds(2 * cq, cv)]),
+        (0, lambda c: wg.at[:, lanes(c, cv)], lambda f: w1.at[rows(f, kb), pl.ds(2 * cq + cv, cv)]),
+        (1, lambda c: wo.at[rows(c, cv), :], lambda f: wout.at[:, lanes(f, nb)]),
+        (2, lambda c: wl.at[:, lanes(c, cf)], lambda f: wlr.at[rows(f, kb), pl.ds(0, cf)]),
+        (2, lambda c: wr.at[:, lanes(c, cf)], lambda f: wlr.at[rows(f, kb), pl.ds(cf, cf)]),
+        (3, lambda c: wd.at[rows(c, cf), :], lambda f: wdown.at[:, lanes(f, nb)]),
+    )
+
+    barrier = pltpu.get_barrier_semaphore()
+    for step in range(1, groups):
+        pl.semaphore_signal(barrier, inc=1, device_id=zdev(zpeer(step)), device_id_type=MESH)
+    for step in range(1, planes):
+        pl.semaphore_signal(barrier, inc=1, device_id=qdev(step), device_id_type=MESH)
+    pl.semaphore_signal(barrier, inc=1, device_id=partner, device_id_type=MESH)
+
+    keeps = []
+    for i, (cls, src, dst) in enumerate(pieces):
+        keep = pltpu.make_async_copy(src(z), dst(fs), self_sem.at[i])
+        keep.start()
+        keeps.append(keep)
+
+    def own_rows(seq, half):
+        return pl.ds(pl.multiple_of(seq * length + half * own, own), own)
+
+    my_half = pl.ds(pl.multiple_of(tp * own, own), own)
+    nt[own_rows(z, tp), :] = normed_rows(tokens[my_half, :].astype(jnp.float32), norm_gain[...])
+    pl.semaphore_wait(barrier, groups - 1 + planes - 1 + 1)
+
+    def remote(src, dst, ssem, rsem, device):
+        return pltpu.make_async_remote_copy(
+            src_ref=src, dst_ref=dst, send_sem=ssem, recv_sem=rsem,
+            device_id=device, device_id_type=MESH,
+        )
+
+    pending = []
+
+    def go(copy):
+        copy.start()
+        pending.append(copy)
+
+    def spread(buf, which):
+        mine = buf.at[own_rows(z, tp), :]
+        for step in range(1, groups):
+            go(remote(mine, mine, a_send.at[which, step], a_recv.at[which, step], zdev(zpeer(step))))
+        go(remote(mine, mine, f_send.at[which, 0], f_recv.at[which, 0], partner))
+
+    def pass_on(buf, which):
+        for step in range(1, groups):
+            got = buf.at[own_rows(zback(step), tp), :]
+            remote(got, got, a_send.at[which, step], a_recv.at[which, step], zdev(zpeer(step))).wait_recv()
+            go(remote(got, got, f_send.at[which, step], f_recv.at[which, step], partner))
+
+    def await_pass(buf, which):
+        for step in range(groups):
+            got = buf.at[own_rows(zback(step), other), :]
+            remote(got, got, f_send.at[which, step], f_recv.at[which, step], partner).wait_recv()
+
+    def first_leg(cls):
+        for step in range(1, groups):
+            for i, (c, src, dst) in enumerate(pieces):
+                if c == cls:
+                    target = zpeer(step)
+                    go(remote(src(target), dst(fs), s1_send.at[i, step], s1_recv.at[i, step], zdev(target)))
+
+    def second_leg(cls, step):
+        f = zback(step) * planes + q
+        for i, (c, src, dst) in enumerate(pieces):
+            if c == cls:
+                if step == 0:
+                    keeps[i].wait()
+                else:
+                    remote(src(z), dst(f), s1_send.at[i, step], s1_recv.at[i, step], zdev(zpeer(step))).wait_recv()
+        for hop in range(1, planes):
+            go(remote(region(cls, f), region(cls, f), s2_send.at[cls, step, hop],
+                      s2_recv.at[cls, step, hop], qdev(hop)))
+
+    def await_leg(cls):
+        for step in range(groups):
+            for hop in range(1, planes):
+                f = zback(step) * planes + lax.rem(q + planes - hop, planes)
+                remote(region(cls, f), region(cls, f), s2_send.at[cls, step, hop],
+                       s2_recv.at[cls, step, hop], qdev(hop)).wait_recv()
+
+    spread(nt, 0)
+    for cls in range(4):
+        first_leg(cls)
+    second_leg(0, 0)
+    second_leg(2, 0)
+    pass_on(nt, 0)
+    for step in range(1, groups):
+        second_leg(0, step)
+    for step in range(groups):
+        second_leg(1, step)
+    await_pass(nt, 0)
+    await_leg(0)
+
+    head = tp * groups + z
+    log_gamma = gammas[pl.ds(head, 1), :]
+    distance = (
+        lax.broadcasted_iota(jnp.int32, (length, length), 0)
+        - lax.broadcasted_iota(jnp.int32, (length, length), 1)
+    ).astype(jnp.float32)
+    decay = jnp.where(distance >= 0, jnp.exp(log_gamma * jnp.maximum(distance, 0.0)), 0.0)
+    chunk = 2 * length if (groups % 2 == 0) else length
+
+    @pl.loop(0, groups * length // chunk)
+    def _(at):
+        span = rows(at, chunk)
+        qkvg[span, :] = jnp.dot(
+            nt[span, :], w1[...], preferred_element_type=jnp.float32
+        ).astype(jnp.bfloat16)
+
+    @pl.loop(0, groups)
+    def _(at):
+        span = rows(at, length)
+        block = qkvg[span, :].astype(jnp.float32)
+
+        def turn(x):
+            return x * cos_t[...] + pltpu.roll(x, cq // 2, 1) * sin_t[...]
+
+        rq = turn(block[:, :cq])
+        rk = turn(block[:, cq : 2 * cq])
+        scores = lax.dot_general(
+            rq, rk, (((1,), (1,)), ((), ())), precision=highest, preferred_element_type=jnp.float32
+        ) * decay
+        kept = jnp.dot(
+            scores, block[:, 2 * cq : 2 * cq + cv], precision=highest,
+            preferred_element_type=jnp.float32,
+        )
+        kept = kept * lax.rsqrt(jnp.mean(kept * kept, axis=-1, keepdims=True) + 1e-06)
+        gain = mixer_gain[:, lanes(z, cv)]
+        hid[span, :] = (kept * gain * silu(block[:, 2 * cq + cv :])).astype(jnp.bfloat16)
+
+    def total(left, weight, part, xb, sb, rb, which):
+        for step in [*range(1, groups), 0]:
+            g = zpeer(step)
+            product = jnp.dot(
+                left[rows(g, length), :], weight[...], preferred_element_type=jnp.float32
+            ).astype(jnp.bfloat16)
+            part[0, g] = product[:own]
+            part[1, g] = product[own:]
+            go(remote(part.at[other, g], xb.at[g], x_send.at[which, step], x_recv.at[which, step], partner))
+        for step in [*range(1, groups), 0]:
+            g = zpeer(step)
+            remote(part.at[other, g], xb.at[g], x_send.at[which, step], x_recv.at[which, step], partner).wait_recv()
+            pair = part[tp, g].astype(jnp.float32) + xb[g].astype(jnp.float32)
+            if step:
+                sb[step] = pair.astype(jnp.bfloat16)
+                go(remote(sb.at[step], rb.at[step], r_send.at[which, step], r_recv.at[which, step], zdev(g)))
+        return pair
+
+    def gather_total(pair, sb, rb, which):
+        for step in range(1, groups):
+            remote(sb.at[step], rb.at[step], r_send.at[which, step], r_recv.at[which, step], zdev(zpeer(step))).wait_recv()
+            pair = pair + rb[step].astype(jnp.float32)
+        return pair
+
+    await_leg(1)
+    pair = total(hid, wout, part1, xb1, sb1, rb1, 0)
+    mid[...] = pair
+    for step in range(1, groups):
+        second_leg(2, step)
+    second_leg(3, 0)
+    middle = (
+        tokens[my_half, :].astype(jnp.float32) + gather_total(mid[...], sb1, rb1, 0)
+    ).astype(jnp.bfloat16).astype(jnp.float32)
+    mid[...] = middle
+    nm[own_rows(z, tp), :] = normed_rows(middle, channel_gain[...])
+    spread(nm, 1)
+    for step in range(1, groups):
+        second_leg(3, step)
+    pass_on(nm, 1)
+    await_pass(nm, 1)
+    await_leg(2)
+
+    @pl.loop(0, groups * length // chunk)
+    def _(at):
+        span = rows(at, chunk)
+        both = jnp.dot(
+            nm[span, :], wlr[...], preferred_element_type=jnp.float32
+        ).astype(jnp.bfloat16).astype(jnp.float32)
+        place = lax.rem(lax.broadcasted_iota(jnp.int32, (chunk, 1), 0), length)
+
+        def convolve(x, taps):
+            count = taps.shape[0]
+            weights = taps[:, lanes(z, cf)]
+            result = x * weights[count - 1 :, :]
+            for back in range(1, count):
+                moved = jnp.where(place >= back, pltpu.roll(x, back, 0), 0.0)
+                result = result + moved * weights[count - 1 - back : count - back, :]
+            return result
+
+        gated[span, :] = (
+            silu(convolve(both[:, :cf], taps_left)) * convolve(both[:, cf:], taps_right)
+        ).astype(jnp.bfloat16)
+
+    await_leg(3)
+    pair = total(gated, wdown, part2, xb2, sb2, rb2, 1)
+    fin[...] = (mid[...] + gather_total(pair, sb2, rb2, 1)).astype(jnp.bfloat16)
+    last = remote(fin, fin_in, o_send, o_recv, partner)
+    last.start()
+    out[my_half, :] = fin[...]
+    last.wait_recv()
+    out[pl.ds(pl.multiple_of(other * own, own), own), :] = fin_in[...]
+    pending.append(last)
+    for copy in pending:
+        copy.wait_send()
+
+
+def body(n_fs, *args):
+    (tokens, norm_gain, w_query, w_key, w_value, w_gate, mixer_gain, w_out, channel_gain,
+     w_left, w_right, taps_left, taps_right, w_down) = args
+    groups = w_query.shape[1] // DK
+    if (
+        groups < 2
+        or n_fs % groups
+        or n_fs == groups
+        or lax.axis_size("tp") != 2
+        or tokens.shape[0] != BLOCK
+        or (w_left.shape[1] // groups) % 128
+        or w_left.shape[1] % groups
+        or w_out.shape[1] % 128
+        or w_query.shape[0] % 16
+    ):
+        return plain_body(*args)
+    length, width = tokens.shape
+    heads = groups * lax.axis_size("tp")
+    cq, cv, cf = w_query.shape[1] // groups, w_value.shape[1] // groups, w_left.shape[1] // groups
+    planes = n_fs // groups
+    own = length // 2
+    cos_t, sin_t = turning(length, DK)
+    vmem = pl.BlockSpec(memory_space=pltpu.VMEM)
+    bf, f32, dma = jnp.bfloat16, jnp.float32, pltpu.SemaphoreType.DMA
+    return pl.pallas_call(
+        functools.partial(layer_kernel, n_fs, groups),
+        out_shape=jax.ShapeDtypeStruct(tokens.shape, bf),
+        in_specs=[vmem] * 17,
+        out_specs=vmem,
+        scratch_shapes=[
+            pltpu.VMEM((width, 2 * cq + 2 * cv), bf),
+            pltpu.VMEM((cv, width), bf),
+            pltpu.VMEM((width, 2 * cf), bf),
+            pltpu.VMEM((cf, width), bf),
+            pltpu.VMEM((groups * length, width), bf),
+            pltpu.VMEM((groups * length, width), bf),
+            pltpu.VMEM((groups * length, 2 * cq + 2 * cv), bf),
+            pltpu.VMEM((groups * length, cv), bf),
+            pltpu.VMEM((groups * length, cf), bf),
+            pltpu.VMEM((2, groups, own, width), bf),
+            pltpu.VMEM((2, groups, own, width), bf),
+            pltpu.VMEM((groups, own, width), bf),
+            pltpu.VMEM((groups, own, width), bf),
+            pltpu.VMEM((groups, own, width), bf),
+            pltpu.VMEM((groups, own, width), bf),
+            pltpu.VMEM((groups, own, width), bf),
+            pltpu.VMEM((groups, own, width), bf),
+            pltpu.VMEM((own, width), f32),
+            pltpu.VMEM((own, width), bf),
+            pltpu.VMEM((own, width), bf),
+            dma((8, groups)),
+            dma((8, groups)),
+            dma((8,)),
+            dma((4, groups, planes)),
+            dma((4, groups, planes)),
+            dma((2, groups)),
+            dma((2, groups)),
+            dma((2, groups)),
+            dma((2, groups)),
+            dma((2, groups)),
+            dma((2, groups)),
+            dma((2, groups)),
+            dma((2, groups)),
+            dma,
+            dma,
+        ],
+        compiler_params=pltpu.CompilerParams(
+            collective_id=0, has_side_effects=True, vmem_limit_bytes=60 * 1024 * 1024
+        ),
+    )(
+        tokens, norm_gain[None], w_query, w_key, w_value, w_gate, mixer_gain[None], w_out,
+        channel_gain[None], w_left, w_right, taps_left, taps_right, w_down,
+        cos_t, sin_t, log_gammas(heads),
+    )
+
+
 def solution(mesh):
     placed = (
         P("fs", None),
@@ -182,4 +597,5 @@
         P(None, "tp"),
         P("tp", "fs"),
     )
-    return jax.shard_map(body, mesh=mesh, in_specs=placed, out_specs=P("fs", None), check_vma=False)
+    return jax.shard_map(
+        functools.partial(body, mesh.shape["fs"]), mesh=mesh, in_specs=placed, out_specs=P("fs", None), check_vma=False)

time: 731 us -> 170 us (0.23)
  the two profiles are of different devices: /device:TPU:0 before, /device:TPU:25 now
where the time goes in v1:
time: 170 us
  Pallas kernels  168 us (99%)
  local copies, waits for them, and re-layouts  1.88 us (1%)
    pallas_call x1, Pallas kernels, body(): pl.pallas_call(functools.partial(layer_kernel, n_fs, groups), out_shape=j...  168 us

profile of v1, /device:TPU:25, one launch (start us, length us, event | category | flops | bytes accessed | tf_op | source)
XLA Modules:
  0.0 169.5 jit_solution(18236546403000160281)
XLA Ops:
  0.0 167.6 %shard_map.163 = bf16[128,2048]{1,0:T(8,128)(2,1)} custom-call(bf16[128,2048]{1,0:T(8,128)(2,1)} %tokens.1, f32[1,2048]{1,0:T(1,128)} %bitcast.3, bf16[128,512]{1,0:T(8,128)(2,1)} %wq.1, bf16[128,512]{1,0:T(8,128)(2,1)} %wk.1, bf16[128,1024]{1,0:T(8,128)(2,1)} %wv.1, bf16[128,1024]{1,0:T(8,128)(2,1)} %wg.1, f32[1,1024]{1,0:T(1,128)} %bitcast.5, ...), custom_call_target="tpu_custom_call" | custom-call | tf_op jit(solution)/shard_map/pallas_call | solution.py:531
  167.6 1.9 %copy.19 = bf16[128,2048]{1,0:T(8,128)(2,1)} copy(bf16[128,2048]{1,0:T(8,128)(2,1)} %shard_map.163) | data formatting | bytes 1048576

commit v2 on v1

--- a/solution.py
+++ b/solution.py
@@ -235,6 +235,8 @@
     rb1,
     rb2,
     mid,
+    acc,
+    both,
     fin,
     fin_in,
     s1_send,
@@ -259,6 +261,9 @@
     other = 1 - tp
     length, width = tokens.shape
     own = length // 2
+    few = own // 2
+    later = range(1, groups)
+    everyone = range(groups)
     kb = wq.shape[0]
     nb = wo.shape[1]
     cq, cv, cf = wq.shape[1] // groups, wv.shape[1] // groups, wl.shape[1] // groups
@@ -271,9 +276,6 @@
 
     def zdev(target):
         return {"fs": target * planes + q, "tp": tp}
-
-    def qdev(step):
-        return {"fs": z * planes + lax.rem(q + step, planes), "tp": tp}
 
     partner = {"fs": fs, "tp": other}
 
@@ -306,8 +308,12 @@
     barrier = pltpu.get_barrier_semaphore()
     for step in range(1, groups):
         pl.semaphore_signal(barrier, inc=1, device_id=zdev(zpeer(step)), device_id_type=MESH)
-    for step in range(1, planes):
-        pl.semaphore_signal(barrier, inc=1, device_id=qdev(step), device_id_type=MESH)
+    qx = q + 1 - 2 * lax.rem(q, 2)
+    qy = q + 2 - 4 * (q // 2)
+    to_x = {"fs": z * planes + qx, "tp": tp}
+    to_y = {"fs": z * planes + qy, "tp": tp}
+    for device in (to_x, to_y):
+        pl.semaphore_signal(barrier, inc=1, device_id=device, device_id_type=MESH)
     pl.semaphore_signal(barrier, inc=1, device_id=partner, device_id_type=MESH)
 
     keeps = []
@@ -321,7 +327,7 @@
 
     my_half = pl.ds(pl.multiple_of(tp * own, own), own)
     nt[own_rows(z, tp), :] = normed_rows(tokens[my_half, :].astype(jnp.float32), norm_gain[...])
-    pl.semaphore_wait(barrier, groups - 1 + planes - 1 + 1)
+    pl.semaphore_wait(barrier, groups - 1 + 2 + 1)
 
     def remote(src, dst, ssem, rsem, device):
         return pltpu.make_async_remote_copy(
@@ -335,22 +341,27 @@
         copy.start()
         pending.append(copy)
 
-    def spread(buf, which):
-        mine = buf.at[own_rows(z, tp), :]
-        for step in range(1, groups):
+    def spread(buf, which, place):
+        mine = buf.at[place(z, tp), :]
+        for step in later:
             go(remote(mine, mine, a_send.at[which, step], a_recv.at[which, step], zdev(zpeer(step))))
         go(remote(mine, mine, f_send.at[which, 0], f_recv.at[which, 0], partner))
 
-    def pass_on(buf, which):
-        for step in range(1, groups):
-            got = buf.at[own_rows(zback(step), tp), :]
+    def pass_on(buf, which, place):
+        for step in later:
+            got = buf.at[place(zback(step), tp), :]
             remote(got, got, a_send.at[which, step], a_recv.at[which, step], zdev(zpeer(step))).wait_recv()
             go(remote(got, got, f_send.at[which, step], f_recv.at[which, step], partner))
 
-    def await_pass(buf, which):
-        for step in range(groups):
-            got = buf.at[own_rows(zback(step), other), :]
+    def await_pass(buf, which, place):
+        for step in everyone:
+            got = buf.at[place(zback(step), other), :]
             remote(got, got, f_send.at[which, step], f_recv.at[which, step], partner).wait_recv()
+
+    def in_half(half):
+        def place(seq, core):
+            return pl.ds(pl.multiple_of(half * groups * own + seq * own + core * few, few), few)
+        return place
 
     def first_leg(cls):
         for step in range(1, groups):
@@ -359,7 +370,18 @@
                     target = zpeer(step)
                     go(remote(src(target), dst(fs), s1_send.at[i, step], s1_recv.at[i, step], zdev(target)))
 
-    def second_leg(cls, step):
+    def half_of(cls, f, half):
+        block = region(cls, f)
+        size = (kb, cv, kb, cf)[cls] // 2
+        return block.at[pl.ds(half * size, size), :]
+
+    hops = ((0, to_x), (1, to_y), (1, to_x), (0, to_y))
+
+    def hop_copy(cls, step, from_q, half, slot, device):
+        ref = half_of(cls, zback(step) * planes + from_q, half)
+        return remote(ref, ref, s2_send.at[cls, step, slot], s2_recv.at[cls, step, slot], device)
+
+    def direct(cls, step):
         f = zback(step) * planes + q
         for i, (c, src, dst) in enumerate(pieces):
             if c == cls:
@@ -367,28 +389,38 @@
                     keeps[i].wait()
                 else:
                     remote(src(z), dst(f), s1_send.at[i, step], s1_recv.at[i, step], zdev(zpeer(step))).wait_recv()
-        for hop in range(1, planes):
-            go(remote(region(cls, f), region(cls, f), s2_send.at[cls, step, hop],
-                      s2_recv.at[cls, step, hop], qdev(hop)))
+        for slot, (half, device) in enumerate(hops):
+            go(hop_copy(cls, step, q, half, slot, device))
+
+    def relay(cls, step):
+        hop_copy(cls, step, qx, 0, 0, to_x).wait_recv()
+        go(hop_copy(cls, step, qx, 0, 4, to_y))
+        hop_copy(cls, step, qy, 1, 1, to_y).wait_recv()
+        go(hop_copy(cls, step, qy, 1, 5, to_x))
 
     def await_leg(cls):
+        diagonal = planes - 1 - q
         for step in range(groups):
-            for hop in range(1, planes):
-                f = zback(step) * planes + lax.rem(q + planes - hop, planes)
-                remote(region(cls, f), region(cls, f), s2_send.at[cls, step, hop],
-                       s2_recv.at[cls, step, hop], qdev(hop)).wait_recv()
-
-    spread(nt, 0)
-    for cls in range(4):
-        first_leg(cls)
-    second_leg(0, 0)
-    second_leg(2, 0)
-    pass_on(nt, 0)
-    for step in range(1, groups):
-        second_leg(0, step)
-    for step in range(groups):
-        second_leg(1, step)
-    await_pass(nt, 0)
+            hop_copy(cls, step, qx, 1, 2, to_x).wait_recv()
+            hop_copy(cls, step, qy, 0, 3, to_y).wait_recv()
+            hop_copy(cls, step, diagonal, 0, 4, to_y).wait_recv()
+            hop_copy(cls, step, diagonal, 1, 5, to_x).wait_recv()
+
+    first_leg(0)
+    spread(nt, 0, own_rows)
+    first_leg(1)
+    first_leg(2)
+    first_leg(3)
+    direct(0, 0)
+    direct(2, 0)
+    relay(0, 0)
+    for step in later:
+        direct(0, step)
+    for step in later:
+        relay(0, step)
+    direct(1, 0)
+    pass_on(nt, 0, own_rows)
+    await_pass(nt, 0, own_rows)
     await_leg(0)
 
     head = tp * groups + z
@@ -406,6 +438,11 @@
         qkvg[span, :] = jnp.dot(
             nt[span, :], w1[...], preferred_element_type=jnp.float32
         ).astype(jnp.bfloat16)
+
+    for step in later:
+        direct(1, step)
+    relay(2, 0)
+    direct(3, 0)
 
     @pl.loop(0, groups)
     def _(at):
@@ -426,80 +463,106 @@
         )
         kept = kept * lax.rsqrt(jnp.mean(kept * kept, axis=-1, keepdims=True) + 1e-06)
         gain = mixer_gain[:, lanes(z, cv)]
-        hid[span, :] = (kept * gain * silu(block[:, 2 * cq + cv :])).astype(jnp.bfloat16)
-
-    def total(left, weight, part, xb, sb, rb, which):
-        for step in [*range(1, groups), 0]:
-            g = zpeer(step)
-            product = jnp.dot(
-                left[rows(g, length), :], weight[...], preferred_element_type=jnp.float32
-            ).astype(jnp.bfloat16)
-            part[0, g] = product[:own]
-            part[1, g] = product[own:]
-            go(remote(part.at[other, g], xb.at[g], x_send.at[which, step], x_recv.at[which, step], partner))
-        for step in [*range(1, groups), 0]:
-            g = zpeer(step)
-            remote(part.at[other, g], xb.at[g], x_send.at[which, step], x_recv.at[which, step], partner).wait_recv()
-            pair = part[tp, g].astype(jnp.float32) + xb[g].astype(jnp.float32)
-            if step:
-                sb[step] = pair.astype(jnp.bfloat16)
-                go(remote(sb.at[step], rb.at[step], r_send.at[which, step], r_recv.at[which, step], zdev(g)))
-        return pair
-
-    def gather_total(pair, sb, rb, which):
-        for step in range(1, groups):
-            remote(sb.at[step], rb.at[step], r_send.at[which, step], r_recv.at[which, step], zdev(zpeer(step))).wait_recv()
-            pair = pair + rb[step].astype(jnp.float32)
-        return pair
-
+        whole = (kept * gain * silu(block[:, 2 * cq + cv :])).astype(jnp.bfloat16)
+        hid[rows(at, own), :] = whole[:own]
+        hid[rows(at + groups, own), :] = whole[own:]
+
+    def multiply(left, weight, part, xb, which, half):
+        value = jnp.dot(
+            left[rows(half, groups * own), :], weight[...], preferred_element_type=jnp.float32
+        ).astype(jnp.bfloat16)
+        for g in everyone:
+            part[half, 0, g] = value[g * own : g * own + few]
+            part[half, 1, g] = value[g * own + few : (g + 1) * own]
+        go(remote(part.at[half, other], xb.at[half], x_send.at[which, half], x_recv.at[which, half], partner))
+
+    def reduce_pair(part, xb, sb, rb, acc, which, half):
+        remote(part.at[half, other], xb.at[half], x_send.at[which, half], x_recv.at[which, half], partner).wait_recv()
+
+        def pair(g):
+            return part[half, tp, g].astype(jnp.float32) + xb[half, g].astype(jnp.float32)
+
+        for step in later:
+            sb[half, step] = pair(zpeer(step)).astype(jnp.bfloat16)
+            go(remote(sb.at[half, step], rb.at[half, step], r_send.at[which, half, step],
+                      r_recv.at[which, half, step], zdev(zpeer(step))))
+        acc[half] = pair(z)
+
+    def collect(sb, rb, acc, which, half):
+        value = acc[half]
+        for step in later:
+            remote(sb.at[half, step], rb.at[half, step], r_send.at[which, half, step],
+                   r_recv.at[which, half, step], zdev(zpeer(step))).wait_recv()
+            value = value + rb[half, step].astype(jnp.float32)
+        return value
+
+    def natural(half, core):
+        return pl.ds(pl.multiple_of(half * own + core * few, few), few)
+
+    for step in everyone:
+        relay(1, step)
     await_leg(1)
-    pair = total(hid, wout, part1, xb1, sb1, rb1, 0)
-    mid[...] = pair
-    for step in range(1, groups):
-        second_leg(2, step)
-    second_leg(3, 0)
-    middle = (
-        tokens[my_half, :].astype(jnp.float32) + gather_total(mid[...], sb1, rb1, 0)
-    ).astype(jnp.bfloat16).astype(jnp.float32)
-    mid[...] = middle
-    nm[own_rows(z, tp), :] = normed_rows(middle, channel_gain[...])
-    spread(nm, 1)
-    for step in range(1, groups):
-        second_leg(3, step)
-    pass_on(nm, 1)
-    await_pass(nm, 1)
-    await_leg(2)
-
-    @pl.loop(0, groups * length // chunk)
-    def _(at):
-        span = rows(at, chunk)
-        both = jnp.dot(
-            nm[span, :], wlr[...], preferred_element_type=jnp.float32
+    multiply(hid, wout, part1, xb1, 0, 0)
+    multiply(hid, wout, part1, xb1, 0, 1)
+    reduce_pair(part1, xb1, sb1, rb1, acc, 0, 0)
+    reduce_pair(part1, xb1, sb1, rb1, acc, 0, 1)
+    for step in later:
+        direct(2, step)
+    for step in later:
+        relay(2, step)
+    for half in range(2):
+        middle = (
+            tokens[natural(half, tp), :].astype(jnp.float32) + collect(sb1, rb1, acc, 0, half)
         ).astype(jnp.bfloat16).astype(jnp.float32)
-        place = lax.rem(lax.broadcasted_iota(jnp.int32, (chunk, 1), 0), length)
-
-        def convolve(x, taps):
-            count = taps.shape[0]
-            weights = taps[:, lanes(z, cf)]
-            result = x * weights[count - 1 :, :]
-            for back in range(1, count):
-                moved = jnp.where(place >= back, pltpu.roll(x, back, 0), 0.0)
-                result = result + moved * weights[count - 1 - back : count - back, :]
-            return result
-
-        gated[span, :] = (
-            silu(convolve(both[:, :cf], taps_left)) * convolve(both[:, cf:], taps_right)
+        mid[half] = middle
+        nm[in_half(half)(z, tp), :] = normed_rows(middle, channel_gain[...])
+        spread(nm, 1 + half, in_half(half))
+    for step in later:
+        direct(3, step)
+    for step in everyone:
+        relay(3, step)
+
+    place = lax.rem(lax.broadcasted_iota(jnp.int32, (groups * own, 1), 0), own)
+
+    def convolve(half, low, taps):
+        x = both[half, :, low : low + cf].astype(jnp.float32)
+        count = taps.shape[0]
+        weights = taps[:, lanes(z, cf)]
+        result = x * weights[count - 1 :, :]
+        for back in range(1, count):
+            if half:
+                before = both[0, :, low : low + cf].astype(jnp.float32)
+                before = pltpu.roll(before, back + (groups - 1) * own, 0)
+            else:
+                before = 0.0
+            moved = jnp.where(place >= back, pltpu.roll(x, back, 0), before)
+            result = result + moved * weights[count - 1 - back : count - back, :]
+        return result
+
+    for half in range(2):
+        pass_on(nm, 1 + half, in_half(half))
+        await_pass(nm, 1 + half, in_half(half))
+        if not half:
+            await_leg(2)
+        both[half] = jnp.dot(
+            nm[rows(half, groups * own), :], wlr[...], preferred_element_type=jnp.float32
         ).astype(jnp.bfloat16)
-
-    await_leg(3)
-    pair = total(gated, wdown, part2, xb2, sb2, rb2, 1)
-    fin[...] = (mid[...] + gather_total(pair, sb2, rb2, 1)).astype(jnp.bfloat16)
-    last = remote(fin, fin_in, o_send, o_recv, partner)
-    last.start()
-    out[my_half, :] = fin[...]
-    last.wait_recv()
-    out[pl.ds(pl.multiple_of(other * own, own), own), :] = fin_in[...]
-    pending.append(last)
+        gated[rows(half, groups * own), :] = (
+            silu(convolve(half, 0, taps_left)) * convolve(half, cf, taps_right)
+        ).astype(jnp.bfloat16)
+        if not half:
+            await_leg(3)
+        multiply(gated, wdown, part2, xb2, 1, half)
+        reduce_pair(part2, xb2, sb2, rb2, acc, 1, half)
+    for half in range(2):
+        mine = natural(half, tp)
+        value = (mid[half] + collect(sb2, rb2, acc, 1, half)).astype(jnp.bfloat16)
+        fin[half] = value
+        go(remote(fin.at[half], fin_in.at[half], o_send.at[half], o_recv.at[half], partner))
+        out[mine, :] = value
+    for half in range(2):
+        remote(fin.at[half], fin_in.at[half], o_send.at[half], o_recv.at[half], partner).wait_recv()
+        out[natural(half, other), :] = fin_in[half]
     for copy in pending:
         copy.wait_send()
 
@@ -511,7 +574,7 @@
     if (
         groups < 2
         or n_fs % groups
-        or n_fs == groups
+        or n_fs != 4 * groups
         or lax.axis_size("tp") != 2
         or tokens.shape[0] != BLOCK
         or (w_left.shape[1] // groups) % 128
@@ -525,13 +588,15 @@
     cq, cv, cf = w_query.shape[1] // groups, w_value.shape[1] // groups, w_left.shape[1] // groups
     planes = n_fs // groups
     own = length // 2
+    few = own // 2
     cos_t, sin_t = turning(length, DK)
     vmem = pl.BlockSpec(memory_space=pltpu.VMEM)
+    held = pl.BlockSpec(memory_space=pl.ANY)
     bf, f32, dma = jnp.bfloat16, jnp.float32, pltpu.SemaphoreType.DMA
     return pl.pallas_call(
         functools.partial(layer_kernel, n_fs, groups),
         out_shape=jax.ShapeDtypeStruct(tokens.shape, bf),
-        in_specs=[vmem] * 17,
+        in_specs=[vmem] * 2 + [held] * 4 + [vmem, held, vmem] + [held] * 2 + [vmem] * 2 + [held] + [vmem] * 3,
         out_specs=vmem,
         scratch_shapes=[
             pltpu.VMEM((width, 2 * cq + 2 * cv), bf),
@@ -543,32 +608,34 @@
             pltpu.VMEM((groups * length, 2 * cq + 2 * cv), bf),
             pltpu.VMEM((groups * length, cv), bf),
             pltpu.VMEM((groups * length, cf), bf),
-            pltpu.VMEM((2, groups, own, width), bf),
-            pltpu.VMEM((2, groups, own, width), bf),
-            pltpu.VMEM((groups, own, width), bf),
-            pltpu.VMEM((groups, own, width), bf),
-            pltpu.VMEM((groups, own, width), bf),
-            pltpu.VMEM((groups, own, width), bf),
-            pltpu.VMEM((groups, own, width), bf),
-            pltpu.VMEM((groups, own, width), bf),
-            pltpu.VMEM((own, width), f32),
-            pltpu.VMEM((own, width), bf),
-            pltpu.VMEM((own, width), bf),
+            pltpu.VMEM((2, 2, groups, few, width), bf),
+            pltpu.VMEM((2, 2, groups, few, width), bf),
+            pltpu.VMEM((2, groups, few, width), bf),
+            pltpu.VMEM((2, groups, few, width), bf),
+            pltpu.VMEM((2, groups, few, width), bf),
+            pltpu.VMEM((2, groups, few, width), bf),
+            pltpu.VMEM((2, groups, few, width), bf),
+            pltpu.VMEM((2, groups, few, width), bf),
+            pltpu.VMEM((2, few, width), f32),
+            pltpu.VMEM((2, few, width), f32),
+            pltpu.VMEM((2, groups * own, 2 * cf), bf),
+            pltpu.VMEM((2, few, width), bf),
+            pltpu.VMEM((2, few, width), bf),
             dma((8, groups)),
             dma((8, groups)),
             dma((8,)),
-            dma((4, groups, planes)),
-            dma((4, groups, planes)),
-            dma((2, groups)),
-            dma((2, groups)),
-            dma((2, groups)),
-            dma((2, groups)),
-            dma((2, groups)),
-            dma((2, groups)),
-            dma((2, groups)),
-            dma((2, groups)),
-            dma,
-            dma,
+            dma((4, groups, 6)),
+            dma((4, groups, 6)),
+            dma((3, groups)),
+            dma((3, groups)),
+            dma((3, groups)),
+            dma((3, groups)),
+            dma((2, 2)),
+            dma((2, 2)),
+            dma((2, 2, groups)),
+            dma((2, 2, groups)),
+            dma((2,)),
+            dma((2,)),
         ],
         compiler_params=pltpu.CompilerParams(
             collective_id=0, has_side_effects=True, vmem_limit_bytes=60 * 1024 * 1024

time: 170 us -> 159 us (0.935)
  the two profiles are of different devices: /device:TPU:25 before, /device:TPU:0 now
where the time goes in v2:
time: 159 us; the launch traced here: 157 us
  Pallas kernels  155 us (97%)
  local copies, waits for them, and re-layouts  1.88 us (1%)
    pallas_call x1, Pallas kernels, body(): pl.pallas_call(functools.partial(layer_kernel, n_fs, groups), out_shape=j...  155 us

profile of v2, /device:TPU:0, one launch (start us, length us, event | category | flops | bytes accessed | tf_op | source)
XLA Modules:
  0.0 156.8 jit_solution(8705208096262288449)
XLA Ops:
  0.0 154.9 %shard_map.163 = bf16[128,2048]{1,0:T(8,128)(2,1)} custom-call(bf16[128,2048]{1,0:T(8,128)(2,1)} %tokens.1, f32[1,2048]{1,0:T(1,128)} %bitcast.3, bf16[128,512]{1,0:T(8,128)(2,1)} %wq.1, bf16[128,512]{1,0:T(8,128)(2,1)} %wk.1, bf16[128,1024]{1,0:T(8,128)(2,1)} %wv.1, bf16[128,1024]{1,0:T(8,128)(2,1)} %wg.1, f32[1,1024]{1,0:T(1,128)} %bitcast.5, ...), custom_call_target="tpu_custom_call" | custom-call | tf_op jit(solution)/shard_map/pallas_call | solution.py:596
  154.9 1.9 %copy.19 = bf16[128,2048]{1,0:T(8,128)(2,1)} copy(bf16[128,2048]{1,0:T(8,128)(2,1)} %shard_map.163) | data formatting | bytes 1048576
